TPU v7x, 512 devices: a 4x2x32 block of a 4x8x32 slice. The times are simulated.
512 devices in a mesh: grp: 2 (over y), kv: 64 (over z, core), tp: 4 (over x).
Axes of the slice: x: 4, y: 2, z: 32, core: 2. Of those that a mesh axis runs over, the one named last changes fastest.
The devices are a block of a 4x8x32 slice.
Arguments:
- piece_rows: bfloat16 [8192, 2048], P(('grp', 'kv')), parts along dimension 0, may hold values from -6 to 6
- dec_rows: bfloat16 [256, 2048], P(('grp', 'kv')), parts along dimension 0, may hold values from -6 to 6
- norm_gain: float32 [2048], replicated, may hold values from 0.1 to 1.9
- w_query: bfloat16 [2048, 1024], P(None, 'tp'), may hold values from -0.25 to 0.25
- w_key: bfloat16 [2048, 256], P(None, 'tp'), may hold values from -0.125 to 0.125
- w_value: bfloat16 [2048, 256], P(None, 'tp'), may hold values from -0.125 to 0.125
- w_forget: bfloat16 [2048, 16], P(None, 'tp'), may hold values from -0.125 to 0.125
- forget_bias: float32 [16], P('tp'), may hold values from 3 to 12
- piece_decay: float32 [16, 8192], P('tp', ('grp', 'kv')), parts along dimension 1, may hold values from -3 to 0
- cache_kv: bfloat16 [98304, 4, 128], P(('grp', 'kv'), 'tp'), parts along dimension 0, may hold values from -150 to 150
- cache_gate: float32 [16, 98304], P('tp', ('grp', 'kv')), parts along dimension 1, may hold values from -2460.6 to 0, as said below
- dec_cache: bfloat16 [256, 3072, 4, 128], P(('grp', 'kv'), None, 'tp'), parts along dimension 0, may hold values from -150 to 150
- dec_gate: float32 [256, 16, 3072], P(('grp', 'kv'), 'tp'), parts along dimension 0, may hold values from -156.6 to 0, as said below
- dec_lengths: int32 [256], P(('grp', 'kv')), parts along dimension 0, may hold values from 1 to 3072, as said below
- w_out: bfloat16 [1024, 2048], P(None, 'tp'), may hold values from -0.75 to 0.75
Outputs:
- piece_out: bfloat16 [8192, 2048], P(('grp', 'kv'), 'tp'), parts along dimension 0
- dec_out: bfloat16 [256, 2048], P(('grp', 'kv'), 'tp'), parts along dimension 0
There are 2 independent parts, one for each index of `grp`. A program takes and returns all parts, laid end to end along the dimension named above; an argument that names none is the same for every part. Nothing has to cross between parts.
Inputs may be any that keep to these rules, and one draw needn't show every extreme that they name: `cache_gate`: each head's values never fall from one position to the next and are 0 at the last cached position. `dec_gate`: each sequence's and head's values never rise from one position to the next. Sequence b's cache holds its first dec_lengths[b] positions; in each part some sequence holds 3072.
All inputs are finite; a program needn't handle non-finite values.
Results may differ from a plain program's by a relative error of at most 0.006.
The roundings to bfloat16 on the way count: a program that leaves them out, or rounds other values in their place, can miss the bound.
Values may be sent and summed in bfloat16 or wider, within the bound.
No kernel may reach another device: no remote copies, remote signals or barrier semaphores. Data moves between devices by JAX's collectives and lax.ppermute only.
A program may use at most 64 MiB of HBM per device.

v0:
```python
import jax
import jax.numpy as jnp
from jax import lax
from jax.sharding import Mesh
from jax.sharding import PartitionSpec as P

KV = ("kv_0", "kv_1")
GRP_KV = ("grp", "kv_0", "kv_1")


def carried_in(array, axis, combine, identity):
    length, mine = (lax.axis_size(axis), lax.axis_index(axis))
    everything = lax.all_gather(array, axis)
    start = jnp.broadcast_to(jnp.asarray(identity, array.dtype), array.shape)

    def lap(k, before):
        reached = k < mine
        new = combine(before, everything[k])
        return jnp.where(reached, new, before)

    return lax.fori_loop(0, length, lap, start)


def in_order(blocks, dim):
    blocks = jnp.moveaxis(blocks, 0, dim)
    lengths = blocks.shape
    return blocks.reshape(*lengths[:dim], lengths[dim] * lengths[dim + 1], *lengths[dim + 2 :])


def stacked_from(array, axes, turns):
    blocks = array
    for k in turns:
        blocks = lax.all_gather(blocks, axes[k])
    done = turns[::-1]
    back = [done.index(k) for k in range(len(axes))]
    blocks = blocks.transpose(*back, *range(len(axes), blocks.ndim))
    return blocks.reshape(-1, *array.shape)


def whole_of(array, axes, turns, dim):
    return in_order(stacked_from(array, axes, turns), dim)


def sent_to_all(array, axis):
    length = lax.axis_size(axis)
    return lax.all_to_all(
        jnp.broadcast_to(array[None], (length, *array.shape)), axis, 0, 0, tiled=True
    )


def gathered_copies(array, axis, dim):
    blocks = sent_to_all(array, axis)
    return in_order(blocks, dim)


def norm_rows(rows, gain):
    wide = rows.astype(jnp.float32)
    scale = lax.rsqrt(jnp.mean(wide * wide, axis=-1, keepdims=True) + 1e-06)
    return (wide * scale * gain).astype(jnp.bfloat16)


def add_terms(earlier, later):
    return earlier + later


def merge_state(state, part):
    peak, total, numer = state
    new_peak, new_total, new_numer = part
    highest = jnp.maximum(peak, new_peak)
    keep = jnp.exp(peak - highest)
    fresh = jnp.exp(new_peak - highest)
    return (
        highest,
        total * keep + new_total * fresh,
        numer * keep[..., None] + new_numer * fresh[..., None],
    )


def group_partial(query, query_index, group_kv, group_bias, group, past_rows, new_rows):
    head_width = query.shape[-1]
    keys = group_kv[..., :head_width]
    values = group_kv[..., head_width:]
    score = jnp.einsum("bkgd,nkd->bkgn", query, keys, preferred_element_type=jnp.float32)
    score = score * head_width ** (-0.5) + group_bias[None]
    rank = jnp.arange(group_kv.shape[0], dtype=jnp.int32)
    new_index = group * new_rows + rank - past_rows
    visible = (rank < past_rows)[None, :] | (new_index[None, :] <= query_index[:, None])
    score = jnp.where(visible[:, None, None, :], score, -jnp.inf)
    peak = jnp.max(score, axis=-1)
    weight = jnp.exp(score - peak[..., None])
    total = jnp.sum(weight, axis=-1)
    numer = jnp.einsum(
        "bkgn,nkd->bkgd", weight.astype(jnp.bfloat16), values, preferred_element_type=jnp.float32
    )
    return (peak, total, numer)


def decode_attention(query, new_key, new_value, new_gate, cache, gate, lengths):
    seqs, pairs_here, group_size, head_width = query.shape
    span = cache.shape[1]
    keys = cache[..., :head_width]
    values = cache[..., head_width:]
    target_location = jnp.arange(span, dtype=jnp.int32)
    last_gate = jnp.sum(
        jnp.where(target_location[None, None, :] == lengths[:, None, None] - 1, gate, 0.0), axis=-1
    )
    score = jnp.einsum(
        "skgd,slkd->skgl", query, keys, preferred_element_type=jnp.float32
    ) * head_width ** (-0.5)
    score = score - gate.reshape(seqs, pairs_here, group_size, span)
    score = jnp.where(
        (target_location[None, :] < lengths[:, None])[:, None, None, :], score, -jnp.inf
    )
    own = jnp.einsum(
        "skgd,skd->skg", query, new_key, preferred_element_type=jnp.float32
    ) * head_width ** (-0.5)
    own = own - (last_gate + new_gate).reshape(seqs, pairs_here, group_size)
    peak = jnp.maximum(jnp.max(score, axis=-1), own)
    weight = jnp.exp(score - peak[..., None])
    own_weight = jnp.exp(own - peak)
    total = jnp.sum(weight, axis=-1) + own_weight
    numer = jnp.einsum(
        "skgl,slkd->skgd", weight.astype(jnp.bfloat16), values, preferred_element_type=jnp.float32
    )
    numer = numer + own_weight.astype(jnp.bfloat16).astype(jnp.float32)[..., None] * new_value[
        :, :, None, :
    ].astype(jnp.float32)
    return numer / total[..., None]


def local(
    piece_rows,
    dec_rows,
    norm_gain,
    w_query,
    w_key,
    w_value,
    w_forget,
    forget_bias,
    piece_decay,
    cache_kv,
    cache_gate,
    dec_cache,
    dec_gate,
    dec_lengths,
    w_out,
):
    piece_count = piece_rows.shape[0]
    dec_count = dec_rows.shape[0]
    past_rows = cache_kv.shape[0]
    pairs_here = cache_kv.shape[1]
    head_width = cache_kv.shape[2] // 2
    heads_here = w_forget.shape[1]
    group_size = heads_here // pairs_here
    group_rows = past_rows + piece_count
    normed = norm_rows(jnp.concatenate([piece_rows, dec_rows], axis=0), norm_gain)
    query = jnp.dot(normed, w_query, preferred_element_type=jnp.float32).astype(jnp.bfloat16)
    new_key = jnp.dot(normed, w_key, preferred_element_type=jnp.float32).astype(jnp.bfloat16)
    new_value = jnp.dot(normed, w_value, preferred_element_type=jnp.float32).astype(jnp.bfloat16)
    log_gate = jax.nn.log_sigmoid(
        jnp.dot(normed, w_forget, preferred_element_type=jnp.float32) + forget_bias
    )
    piece_gate = log_gate[:piece_count] + piece_decay.T
    running = jnp.cumsum(piece_gate, axis=0)
    before = carried_in(running[-1], KV, add_terms, jnp.zeros((heads_here,), jnp.float32))
    new_bias = -(running + before[None, :]).T
    piece_kv = jnp.concatenate(
        [
            new_key[:piece_count].reshape(piece_count, pairs_here, head_width),
            new_value[:piece_count].reshape(piece_count, pairs_here, head_width),
        ],
        axis=-1,
    )
    group_kv = jnp.concatenate([cache_kv, piece_kv], axis=0)
    group_bias = jnp.concatenate([cache_gate, new_bias], axis=1)
    my_group = lax.axis_index(KV)
    every_bias = whole_of(group_bias, KV, (0, 1), 1)
    own_query = query[:piece_count].reshape(piece_count, pairs_here, group_size, head_width)
    own_index = my_group * piece_count + jnp.arange(piece_count, dtype=jnp.int32)
    start_state = (
        jnp.full((piece_count, pairs_here, group_size), -jnp.inf, jnp.float32),
        jnp.zeros((piece_count, pairs_here, group_size), jnp.float32),
        jnp.zeros((piece_count, pairs_here, group_size, head_width), jnp.float32),
    )
    state = start_state
    piece = lax.all_gather(group_kv, KV, axis=0, tiled=True)
    count = piece.shape[0] // group_rows
    blocks = piece.reshape(count, group_rows, pairs_here, 2 * head_width)

    def visit(carry, item):
        block, offset = item
        bias = lax.dynamic_slice_in_dim(every_bias, offset * group_rows, group_rows, 1)
        part = group_partial(
            own_query,
            own_index,
            block,
            bias.reshape(pairs_here, group_size, group_rows),
            offset,
            past_rows,
            piece_count,
        )
        return (merge_state(carry, part), None)

    state, _ = lax.scan(visit, state, (blocks, jnp.arange(count, dtype=jnp.int32)))
    peak, total, numer = state
    piece_attn = numer / total[..., None]
    dec_attn = decode_attention(
        query[piece_count:].reshape(dec_count, pairs_here, group_size, head_width),
        new_key[piece_count:].reshape(dec_count, pairs_here, head_width),
        new_value[piece_count:].reshape(dec_count, pairs_here, head_width),
        log_gate[piece_count:],
        dec_cache,
        dec_gate,
        dec_lengths,
    )
    attn_rows = jnp.concatenate(
        [
            piece_attn.reshape(piece_count, heads_here * head_width),
            dec_attn.reshape(dec_count, heads_here * head_width),
        ],
        axis=0,
    ).astype(jnp.bfloat16)
    every_head = gathered_copies(attn_rows, "tp", 1)
    mixed = jnp.dot(every_head, w_out, preferred_element_type=jnp.float32).astype(jnp.bfloat16)
    return (mixed[:piece_count], mixed[piece_count:])


def solution(mesh):
    finer = Mesh(
        mesh.devices.reshape(mesh.shape["grp"], 32, 2, mesh.shape["tp"]),
        ("grp", "kv_0", "kv_1", "tp"),
    )
    return jax.shard_map(
        local,
        mesh=finer,
        in_specs=(
            P(GRP_KV, None),
            P(GRP_KV, None),
            P(),
            P(None, "tp"),
            P(None, "tp"),
            P(None, "tp"),
            P(None, "tp"),
            P("tp"),
            P("tp", GRP_KV),
            P(GRP_KV, "tp", None),
            P("tp", GRP_KV),
            P(GRP_KV, None, "tp", None),
            P(GRP_KV, "tp", None),
            P(GRP_KV),
            P(None, "tp"),
        ),
        out_specs=(P(GRP_KV, "tp"), P(GRP_KV, "tp")),
        check_vma=False,
    )
```

profile of v0, /device:TPU:33, one launch (start us, length us, event | category | flops | bytes accessed | tf_op | source)
XLA Modules:
  0.0 496.2 jit_solution(10533658309555598775)
XLA Ops:
  7.3 1.2 fusion.35
  8.6 1.4 convolution_convert_fusion.2
  10.0 1.4 convolution_convert_fusion.3
  12.3 1.7 convolution_convert_fusion.1
  14.9 96.8 %all-gather.2 = f32[64,1,4]{2,1,0:T(1,128)S(1)} all-gather(f32[1,1,4]{2,1,0:T(1,128)S(1)} %slice_bitcast_fusion.7), channel_id=1, replica_groups=mesh['grp'=2,'kv_0'=32,'kv_1'=2,'tp'=4] {'kv_0','kv_1'}, dimensions={0}, use_global_device_ids=true | all-gather | bytes 1040 | tf_op jit(solution)/shard_map/all_gather | solution.py:13
  111.8 2.6 while.31
  117.1 46.0 %all-gather.3 = f32[32,4,832]{2,1,0:T(4,128)S(1)} all-gather(f32[1,4,832]{2,1,0:T(4,128)S(1)} %maximum_bitcast_fusion), channel_id=2, replica_groups=mesh['grp'=2,'kv_0'=32,'kv_1'=2,'tp'=4] {'kv_0'}, dimensions={0}, use_global_device_ids=true | all-gather | bytes 439296 | tf_op jit(solution)/shard_map/all_gather | solution.py:33
  163.1 11.7 %all-gather.1 = f32[64,4,832]{2,1,0:T(4,128)S(1)} all-gather(f32[32,4,832]{2,1,0:T(4,128)S(1)} %all-gather.3), channel_id=3, replica_groups=mesh['grp'=2,'kv_0'=32,'kv_1'=2,'tp'=4] {'kv_1'}, dimensions={0}, use_global_device_ids=true | all-gather | bytes 1277952 | tf_op jit(solution)/shard_map/all_gather | solution.py:33
  175.6 12.4 %all-gather.6.cloned.1.call-done = bf16[53248,1,128]{2,0,1:T(8,128)(2,1)} async-done(((bf16[832,1,128]{2,0,1:T(8,128)(2,1)}), bf16[53248,1,128]{2,0,1:T(8,128)(2,1)}) %all-gather.6.cloned.1.call-update) | async-done | bytes 13631504 | tf_op jit(solution)/shard_map/all_gather | solution.py:186
  188.0 290.5 %while.32 = (s32[]{:T(128)}, f32[64,1,4]{0,2,1:T(4,128)S(1)}, f32[64,1,4]{0,2,1:T(4,128)S(1)}, f32[64,1,4,64]{0,3,2,1:T(8,128)S(1)}, s32[64]{0:T(128)S(1)}, /*in...) while((s32[]{:T(128)}, f32[64,1,4]{0,2,1:T(4,128)S(1)}, ...), condition=%wide.region_7.8_spmd.clone, body=%wide.region_4.7_spmd.clone.sunk | while | flops 56406536 | bytes 4148079 | solution.py:204
  190.1 1.0 constant_dynamic-slice_fusion.5
  194.7 1.0 constant_dynamic-slice_fusion.5
  199.2 1.0 constant_dynamic-slice_fusion.5
  203.7 1.0 constant_dynamic-slice_fusion.5
  208.3 1.0 constant_dynamic-slice_fusion.5
  212.8 1.0 constant_dynamic-slice_fusion.5
  217.4 1.0 constant_dynamic-slice_fusion.5
  221.9 1.0 constant_dynamic-slice_fusion.5
  226.4 1.0 constant_dynamic-slice_fusion.5
  231.0 1.0 constant_dynamic-slice_fusion.5
  267.3 1.0 constant_dynamic-slice_fusion.5
  280.9 1.0 constant_dynamic-slice_fusion.5
  303.6 1.0 constant_dynamic-slice_fusion.5
  317.2 1.0 constant_dynamic-slice_fusion.5
  353.5 1.0 constant_dynamic-slice_fusion.5
  367.1 1.0 constant_dynamic-slice_fusion.5
  389.8 1.0 constant_dynamic-slice_fusion.5
  403.5 1.0 constant_dynamic-slice_fusion.5
  439.8 1.0 constant_dynamic-slice_fusion.5
  453.4 1.0 constant_dynamic-slice_fusion.5
  476.1 1.0 constant_dynamic-slice_fusion.5
  478.6 9.1 %all_to_all.5 = bf16[4,66,256]{2,1,0:T(8,128)(2,1)S(1)} all-to-all(bf16[4,66,256]{2,1,0:T(8,128)(2,1)S(1)} %broadcast_in_dim.84), channel_id=1, replica_groups=mesh['grp'=2,'kv_0'=32,'kv_1'=2,'tp'=4] {'tp'}, dimensions={0} | all-to-all | bytes 270336 | tf_op jit(solution)/shard_map/all_to_all | solution.py:46
  (1019 shorter events, 189.9 us)
Async XLA Ops:
  7.2 480.7 %copy-start = (bf16[1024,512]{1,0:T(8,128)(2,1)S(1)}, bf16[1024,512]{1,0:T(8,128)(2,1)}, u32[]{:S(2)}) copy-start(bf16[1024,512]{1,0:T(8,128)(2,1)} %param.33) | copy-start | bytes 3145732
  7.2 5.1 %copy-start.6 = (bf16[2,2048]{1,0:T(2,128)(2,1)S(1)}, bf16[2,2048]{1,0:T(2,128)(2,1)}, u32[]{:S(2)}) copy-start(bf16[2,2048]{1,0:T(2,128)(2,1)} %param.20) | copy-start | bytes 24580
  7.2 5.1 %copy-start.3 = (bf16[64,2048]{1,0:T(8,128)(2,1)S(1)}, bf16[64,2048]{1,0:T(8,128)(2,1)}, u32[]{:S(2)}) copy-start(bf16[64,2048]{1,0:T(8,128)(2,1)} %param.19) | copy-start | bytes 786436
  7.2 5.1 %copy-start.10 = (f32[2048]{0:T(1024)S(1)}, f32[2048]{0:T(1024)}, u32[]{:S(2)}) copy-start(f32[2048]{0:T(1024)} %param.21) | copy-start | bytes 24580
  7.2 4.2 copy-start.4
  7.2 180.8 %all-gather.6.cloned.1.call-start = ((), (), s32[]{:S(2)}) async-start(), calls=%async_computation.1 | async-start | bytes 13844480 | tf_op jit(solution)/shard_map/all_gather | solution.py:186
  9.9 4.1 copy-start.8
  9.9 4.2 copy-start.2
  10.0 4.4 copy-start.9
  10.0 4.4 copy-start.11
  11.4 3.3 copy-start.7
  12.3 102.6 %copy-start.1 = (bf16[2,3072,1,128]{3,1,2,0:T(8,128)(2,1)S(1)}, bf16[2,3072,1,128]{3,1,2,0:T(8,128)(2,1)}, u32[]{:S(2)}) copy-start(bf16[2,3072,1,128]{3,1,2,0:T(8,128)(2,1)} %param.30) | copy-start | bytes 4718596
  115.0 2.1 copy-start.5
Sparse Core Ops, SparseCore 0:
  12.4 175.5 all-gather.5
where the time goes:
time: 499 us; the launch traced here: 496 us
  blocking collectives  164 us (33%)
  local copies, waits for them, and re-layouts  118 us (24%)
  loops' own time  90.1 us (18%)
  matrix products  64.2 us (13%)
  other arithmetic  33.3 us (7%)
  between operations  14.5 us (3%)
  waiting for transfers between devices  12.5 us (3%)
    dynamic_slice x192, local copies, waits for them, and re-layouts, local(): lax.scan(visit, state, (blocks, jnp.arange(count, dtype=jnp.int32)))  109 us
    all_gather x1, blocking collectives, carried_in(): everything = lax.all_gather(array, axis)  96.8 us
    another operation x1, loops' own time, local(): lax.scan(visit, state, (blocks, jnp.arange(count, dtype=jnp.int32)))  88.6 us
    all_gather x2, blocking collectives, stacked_from(): blocks = lax.all_gather(blocks, axes[k])  57.7 us
    dot_general x64, matrix products, group_partial(): jnp.einsum('bkgn,nkd->bkgd', weight.astype(jnp.bfloat16), values, preferr...  33.8 us
    dot_general x64, matrix products, group_partial(): jnp.einsum('bkgd,nkd->bkgn', query, keys, preferred_element_type=jnp.floa...  24 us
    reduce_sum x64, other arithmetic, group_partial(): total = jnp.sum(weight, axis=-1)  19.4 us
    all_gather x1, waiting for transfers between devices, local(): piece = lax.all_gather(group_kv, KV, axis=0, tiled=True)  12.4 us
  transfers between devices with their start and end apart: 1, of which 1 were waited for; matrix products, arithmetic and copies ran while one was open for 1% of the time, Pallas kernels for 0%

commit v1 on v0

--- a/solution.py
+++ b/solution.py
@@ -3,6 +3,7 @@
 from jax import lax
 from jax.sharding import Mesh
 from jax.sharding import PartitionSpec as P
+from jax.lax import all_to_all, axis_size
 
 KV = ("kv_0", "kv_1")
 GRP_KV = ("grp", "kv_0", "kv_1")
@@ -183,7 +184,9 @@
         jnp.zeros((piece_count, pairs_here, group_size, head_width), jnp.float32),
     )
     state = start_state
-    piece = lax.all_gather(group_kv, KV, axis=0, tiled=True)
+    piece = jnp.concatenate(
+        all_to_all(jnp.stack([group_kv] * axis_size(KV), axis=0), KV, 0, 0), axis=0
+    )
     count = piece.shape[0] // group_rows
     blocks = piece.reshape(count, group_rows, pairs_here, 2 * head_width)
 

time: 499 us -> 1660 us (3.33)
  blocking collectives: 164 us -> 1280 us
  starting transfers between devices: 0.06 us -> 47.6 us
    all_gather x1, blocking collectives: 96.8 us -> 1220 us  [carried_in(): everything = lax.all_gather(array, axis)]
    all_to_all x0 -> x1, starting transfers between devices: none -> 47.6 us  [local(): all_to_all(jnp.stack([group_kv] * axis_size(KV), axis=0), KV, 0, 0)]
  transfers between devices with their start and end apart: 1 -> 1, of which waited for: 1 -> 0; matrix products, arithmetic and copies ran while one was open for 1% -> 0% of each run, Pallas kernels for 0% -> 0%
where the time goes in v1:
time: 1660 us; the launch traced here: 1650 us
  blocking collectives  1280 us (77%)
  local copies, waits for them, and re-layouts  130 us (8%)
  loops' own time  94.1 us (6%)
  matrix products  64.4 us (4%)
  starting transfers between devices  47.6 us (3%)
  other arithmetic  31.9 us (2%)
    all_gather x1, blocking collectives, carried_in(): everything = lax.all_gather(array, axis)  1220 us
    dynamic_slice x192, local copies, waits for them, and re-layouts, local(): lax.scan(visit, state, (blocks, jnp.arange(count, dtype=jnp.int32)))  113 us
    another operation x1, loops' own time, local(): lax.scan(visit, state, (blocks, jnp.arange(count, dtype=jnp.int32)))  92.6 us
    all_gather x2, blocking collectives, stacked_from(): blocks = lax.all_gather(blocks, axes[k])  56.6 us
    all_to_all x1, starting transfers between devices, local(): all_to_all(jnp.stack([group_kv] * axis_size(KV), axis=0), KV, 0, 0)  47.6 us
    dot_general x64, matrix products, group_partial(): jnp.einsum('bkgn,nkd->bkgd', weight.astype(jnp.bfloat16), values, preferr...  33.9 us
  transfers between devices with their start and end apart: 1, of which 0 were waited for; matrix products, arithmetic and copies ran while one was open for 0% of the time, Pallas kernels for 0%

profile of v1, /device:TPU:33, one launch (start us, length us, event | category | flops | bytes accessed | tf_op | source)
XLA Modules:
  0.0 1652.7 jit_solution(13143176417820395110)
XLA Ops:
  0.7 1.2 fusion.35
  1.9 1.4 convolution_convert_fusion.3
  3.3 1.4 convolution_convert_fusion.2
  4.8 8.2 stack.2
  13.0 47.6 %all-to-all-start = ((bf16[64,832,1,128]{3,1,2,0:T(8,128)(2,1)}), bf16[64,832,1,128]{3,1,2,0:T(8,128)(2,1)}, u32[]{:S(2)}, u32[]{:S(2)}) async-start(bf16[64,832,1,128]{3,1,2,0:T(8,128)(2,1)} %stack.2), calls=%async_computation | async-start | bytes 27262976 | tf_op jit(solution)/shard_map/all_to_all | solution.py:188
  60.7 1.7 convolution_convert_fusion.1
  65.7 1216.4 %all-gather.2 = f32[64,1,4]{2,1,0:T(1,128)S(1)} all-gather(f32[1,1,4]{2,1,0:T(1,128)S(1)} %slice_bitcast_fusion.7), channel_id=1, replica_groups=mesh['grp'=2,'kv_0'=32,'kv_1'=2,'tp'=4] {'kv_0','kv_1'}, dimensions={0}, use_global_device_ids=true | all-gather | bytes 1040 | tf_op jit(solution)/shard_map/all_gather | solution.py:14
  1282.1 2.6 while.31
  1284.8 40.9 %all-gather.3 = f32[32,4,832]{2,1,0:T(4,128)S(1)} all-gather(f32[1,4,832]{2,1,0:T(4,128)S(1)} %maximum_bitcast_fusion.1), channel_id=2, replica_groups=mesh['grp'=2,'kv_0'=32,'kv_1'=2,'tp'=4] {'kv_0'}, dimensions={0}, use_global_device_ids=true | all-gather | bytes 439296 | tf_op jit(solution)/shard_map/all_gather | solution.py:34
  1325.7 15.7 all-gather.1
  1342.4 297.9 %while.32 = (s32[]{:T(128)}, f32[64,1,4]{0,2,1:T(4,128)S(1)}, f32[64,1,4]{0,2,1:T(4,128)S(1)}, f32[64,1,4,64]{0,3,2,1:T(8,128)S(1)}, s32[64]{0:T(128)S(1)}, /*in...) while((s32[]{:T(128)}, f32[64,1,4]{0,2,1:T(4,128)S(1)}, ...), condition=%wide.region_7.8_spmd.clone, body=%wide.region_4.7_spmd.clone.sunk | while | flops 56406536 | bytes 4148071 | solution.py:207
  1344.6 1.0 constant_dynamic-slice_fusion.5
  1349.3 1.0 constant_dynamic-slice_fusion.5
  1353.9 1.0 constant_dynamic-slice_fusion.5
  1358.6 1.0 constant_dynamic-slice_fusion.5
  1363.2 1.0 constant_dynamic-slice_fusion.5
  1367.9 1.0 constant_dynamic-slice_fusion.5
  1372.5 1.0 constant_dynamic-slice_fusion.5
  1377.2 1.0 constant_dynamic-slice_fusion.5
  1381.9 1.0 constant_dynamic-slice_fusion.5
  1386.5 1.0 constant_dynamic-slice_fusion.5
  1391.2 1.0 constant_dynamic-slice_fusion.5
  1437.7 1.0 constant_dynamic-slice_fusion.5
  1447.0 1.0 constant_dynamic-slice_fusion.5
  1479.6 1.0 constant_dynamic-slice_fusion.5
  1493.6 1.0 constant_dynamic-slice_fusion.5
  1526.2 1.0 constant_dynamic-slice_fusion.5
  1535.5 1.0 constant_dynamic-slice_fusion.5
  1582.0 1.0 constant_dynamic-slice_fusion.5
  1586.7 1.0 constant_dynamic-slice_fusion.5
  1596.0 1.0 constant_dynamic-slice_fusion.5
  1640.4 10.6 all_to_all.10
  (1022 shorter events, 193.6 us)
Async XLA Ops:
  0.6 1650.5 %copy-start = (bf16[1024,512]{1,0:T(8,128)(2,1)S(1)}, bf16[1024,512]{1,0:T(8,128)(2,1)}, u32[]{:S(2)}) copy-start(bf16[1024,512]{1,0:T(8,128)(2,1)} %param.33) | copy-start | bytes 3145732
  0.6 4.0 copy-start.4
  12.9 47.7 %copy-start.3 = (bf16[64,2048]{1,0:T(8,128)(2,1)S(1)}, bf16[64,2048]{1,0:T(8,128)(2,1)}, u32[]{:S(2)}) copy-start(bf16[64,2048]{1,0:T(8,128)(2,1)} %param.19) | copy-start | bytes 786436
  12.9 47.7 %copy-start.7 = (bf16[2,2048]{1,0:T(2,128)(2,1)S(1)}, bf16[2,2048]{1,0:T(2,128)(2,1)}, u32[]{:S(2)}) copy-start(bf16[2,2048]{1,0:T(2,128)(2,1)} %param.20) | copy-start | bytes 24580
  13.0 47.7 %copy-start.11 = (f32[2048]{0:T(1024)S(1)}, f32[2048]{0:T(1024)}, u32[]{:S(2)}) copy-start(f32[2048]{0:T(1024)} %param.21) | copy-start | bytes 24580
  13.0 49.8 %copy-start.2 = (f32[2,4,3072]{2,1,0:T(4,128)S(1)}, f32[2,4,3072]{2,1,0:T(4,128)}, u32[]{:S(2)}) copy-start(f32[2,4,3072]{2,1,0:T(4,128)} %param.31) | copy-start | bytes 294916
  13.0 1329.4 %all-to-all-start = ((bf16[64,832,1,128]{3,1,2,0:T(8,128)(2,1)}), bf16[64,832,1,128]{3,1,2,0:T(8,128)(2,1)}, u32[]{:S(2)}, u32[]{:S(2)}) async-start(bf16[64,832,1,128]{3,1,2,0:T(8,128)(2,1)} %stack.2), calls=%async_computation | async-start | bytes 27262976 | tf_op jit(solution)/shard_map/all_to_all | solution.py:188
  60.6 2.1 copy-start.9
  60.6 2.2 copy-start.1
  60.6 3.2 copy-start.10
  60.6 3.2 copy-start.12
  62.3 3.1 copy-start.5
  63.4 2.1 copy-start.8
  63.7 1221.0 %copy-start.6 = (f32[4,768]{1,0:T(4,128)S(1)}, f32[4,768]{1,0:T(4,128)}, u32[]{:S(2)}) copy-start(f32[4,768]{1,0:T(4,128)} %param.29) | copy-start | bytes 36868
  1341.5 0.8 slice-start
